TPU v7x, 256 devices: a whole 4x4x8 slice. The times are simulated.
256 devices in a mesh: rep: 2 (over z_hi), fs: 16 (over z_lo, x), tp: 8 (over y, core).
Axes of the slice: x: 4, y: 4, z: 8 (z_hi: 2, z_lo: 4; z = z_hi * 4 + z_lo), core: 2. Of those that a mesh axis runs over, the one named last changes fastest.
Arguments:
- tokens: bfloat16 [24576, 2048], P(('rep', 'fs'), 'tp'), parts along dimension 0, may hold values from -6 to 6
- mixer_gain: float32 [2048], replicated, may hold values from 0.1 to 1.9
- rec_weight: bfloat16 [2048, 2048], P('fs', 'tp'), may hold values from -0.125 to 0.125
- gate_weight: bfloat16 [2048, 2048], P('fs', 'tp'), may hold values from -0.125 to 0.125
- conv_taps: bfloat16 [4, 2048], P(None, 'tp'), may hold values from -3 to 3
- recur_map: bfloat16 [8, 256, 256], P('tp'), may hold values from -0.375 to 0.375
- input_map: bfloat16 [8, 256, 256], P('tp'), may hold values from -0.375 to 0.375
- decay_param: float32 [2048], P('tp'), may hold values from 3 to 11
- out_weight: bfloat16 [2048, 2048], P('tp', 'fs'), may hold values from -0.5 to 0.5
- mlp_gain: float32 [2048], replicated, may hold values from 0.1 to 1.9
- up_weight: bfloat16 [2048, 8192], P('fs', 'tp'), may hold values from -0.125 to 0.125
- down_weight: bfloat16 [8192, 2048], P('tp', 'fs'), may hold values from -0.0625 to 0.0625
Outputs:
- layer_out: bfloat16 [24576, 2048], P(('rep', 'fs'), 'tp'), parts along dimension 0
There are 2 independent parts, one for each index of `rep`. A program takes and returns all parts, laid end to end along the dimension named above; an argument that names none is the same for every part. Nothing has to cross between parts.
All inputs are finite; a program needn't handle non-finite values.
Results may differ from a plain program's by a relative error of at most 0.022.
Values may be sent and summed in bfloat16 or wider, within the bound.
A program may use at most 64 MiB of HBM per device.

v0:
```python
import jax
import jax.numpy as jnp
from jax import lax
from jax.sharding import PartitionSpec as P

NORM_EPSILON = 1e-06
GATE_SCALE = 8.0


def turned_gather(arrays, axis, dims):
    turned = [jnp.moveaxis(a, dim, 0) for a, dim in zip(arrays, dims)]
    widths = [t[0].size for t in turned]
    both = jnp.concatenate([t.reshape(-1, w) for t, w in zip(turned, widths)], axis=1)
    filled = lax.all_gather(both, axis, axis=0, tiled=True)
    blocks = jnp.split(filled, [sum(widths[:k]) for k in range(1, len(widths))], axis=1)
    return tuple(
        (
            jnp.moveaxis(b.reshape(-1, *t.shape[1:]), 0, dim)
            for b, t, dim in zip(blocks, turned, dims)
        )
    )


def joined_along(blocks, dim):
    blocks = jnp.moveaxis(blocks, 0, dim)
    lengths = blocks.shape
    return blocks.reshape(*lengths[:dim], lengths[dim] * lengths[dim + 1], *lengths[dim + 2 :])


def from_everyone(array, axis):
    copies = jnp.broadcast_to(array, (lax.axis_size(axis), *array.shape))
    return lax.all_to_all(copies, axis, split_axis=0, concat_axis=0, tiled=True)


def gather_directly(array, axis, dim):
    return joined_along(from_everyone(array, axis), dim)


def side_by_side(arrays, axis, dim, along):
    ends, at = ([], 0)
    for a in arrays[:-1]:
        at += a.shape[along]
        ends.append(at)
    both = jnp.concatenate(arrays, axis=along)
    return tuple(jnp.split(lax.all_gather(both, axis, axis=dim, tiled=True), ends, axis=along))


def cut_along(array, dim, count):
    lengths = array.shape
    blocks = array.reshape(*lengths[:dim], count, lengths[dim] // count, *lengths[dim + 1 :])
    return jnp.moveaxis(blocks, dim, 0)


def sent_and_summed(array, axis, dim):
    blocks = cut_along(array, dim, lax.axis_size(axis))
    arrived = lax.all_to_all(blocks, axis, split_axis=0, concat_axis=0, tiled=True)
    return arrived.astype(jnp.float32).sum(axis=0)


def rms_rows(full_rows, gain):
    widened = full_rows.astype(jnp.float32)
    inverse = lax.rsqrt(jnp.mean(widened * widened, axis=-1, keepdims=True) + NORM_EPSILON)
    return (widened * inverse * gain).astype(jnp.bfloat16)


def causal_taps(branch, conv_taps):
    widened = branch.astype(jnp.float32)
    tap_values = conv_taps.astype(jnp.float32)
    tap_count = tap_values.shape[0]
    length = widened.shape[0]
    padded = jnp.pad(widened, ((tap_count - 1, 0), (0, 0)))
    running = jnp.zeros_like(widened)
    for offset in range(tap_count):
        running = running + padded[offset : offset + length, :] * tap_values[offset]
    return running.astype(jnp.bfloat16)


def combine(earlier, latter):
    return (earlier[0] * latter[0], latter[0] * earlier[1] + latter[1])


def add_rows(operand, column_piece):
    return jnp.dot(operand, column_piece, preferred_element_type=jnp.float32)


def feature_term(whole_weight, hidden):
    return lax.dot_general(
        whole_weight, hidden, (((0,), (1,)), ((), ())), preferred_element_type=jnp.float32
    )


def recurrence(branch, gate_branch, conv_taps, recur_map, input_map, decay_param):
    length = branch.shape[0]
    block_w = recur_map.shape[1]
    conv_out = causal_taps(branch, conv_taps)
    blocks = conv_out.reshape(length, -1, block_w)
    recur_gate = jax.nn.sigmoid(
        jnp.einsum("lnc,ncd->lnd", blocks, recur_map, preferred_element_type=jnp.float32).reshape(
            length, -1
        )
    )
    input_gate = jax.nn.sigmoid(
        jnp.einsum("lnc,ncd->lnd", blocks, input_map, preferred_element_type=jnp.float32).reshape(
            length, -1
        )
    )
    log_decay = -GATE_SCALE * recur_gate * jax.nn.softplus(-decay_param)
    decay_rate = jnp.exp(log_decay)
    drive_term = jnp.sqrt(-jnp.expm1(2.0 * log_decay)) * (input_gate * conv_out.astype(jnp.float32))
    _, states = lax.associative_scan(combine, (decay_rate, drive_term), axis=0)
    return (states * jax.nn.gelu(gate_branch.astype(jnp.float32))).astype(jnp.bfloat16)


def shards(
    tokens,
    mixer_gain,
    rec_weight,
    gate_weight,
    conv_taps,
    recur_map,
    input_map,
    decay_param,
    out_weight,
    mlp_gain,
    up_weight,
    down_weight,
):
    up_whole, down_whole = turned_gather((up_weight, down_weight), "fs", (0, 1))
    full_rows = gather_directly(tokens, "tp", 1)
    normed = rms_rows(full_rows, mixer_gain)
    pieces = side_by_side((rec_weight, gate_weight), "fs", 0, 1)
    branch_sum = add_rows(normed, pieces[0])
    gate_sum = add_rows(normed, pieces[1])
    branch = branch_sum.astype(jnp.bfloat16)
    gate_branch = gate_sum.astype(jnp.bfloat16)
    mixed_out = recurrence(branch, gate_branch, conv_taps, recur_map, input_map, decay_param)
    out_whole = gather_directly(out_weight, "fs", 1)
    mixer_out = sent_and_summed(feature_term(out_whole, mixed_out).astype(jnp.bfloat16), "tp", 0).T
    middle = (tokens.astype(jnp.float32) + mixer_out).astype(jnp.bfloat16)
    middle_rows = gather_directly(middle, "tp", 1)
    normed_mlp = rms_rows(middle_rows, mlp_gain)
    lifted = jnp.dot(normed_mlp, up_whole, preferred_element_type=jnp.float32)
    squared = jnp.square(jax.nn.relu(lifted)).astype(jnp.bfloat16)
    mlp_out = sent_and_summed(feature_term(down_whole, squared).astype(jnp.bfloat16), "tp", 0).T
    return (middle.astype(jnp.float32) + mlp_out).astype(jnp.bfloat16)


def solution(mesh):
    placed = (
        P(("rep", "fs"), "tp"),
        P(),
        P("fs", "tp"),
        P("fs", "tp"),
        P(None, "tp"),
        P("tp", None, None),
        P("tp", None, None),
        P("tp"),
        P("tp", "fs"),
        P(),
        P("fs", "tp"),
        P("tp", "fs"),
    )
    return jax.shard_map(
        shards, mesh=mesh, in_specs=placed, out_specs=P(("rep", "fs"), "tp"), check_vma=False
    )
```

profile of v0, /device:TPU:6, one launch (start us, length us, event | category | flops | bytes accessed | tf_op | source)
XLA Modules:
  0.0 285.1 jit_solution(8443693442468253675)
XLA Ops:
  6.5 1.6 pad_maximum_fusion.3
  8.1 1.2 copy.24
  9.3 1.9 broadcast_in_dim.6
  11.2 4.6 %all-to-all-start = ((bf16[8,768,256]{1,2,0:T(8,128)(2,1)}), bf16[8,768,256]{1,2,0:T(8,128)(2,1)S(1)}, u32[]{:S(2)}, u32[]{:S(2)}) async-start(bf16[8,768,256]{1,2,0:T(8,128)(2,1)} %broadcast_in_dim.6), calls=%async_computation | async-start | bytes 6291456 | tf_op jit(solution)/shard_map/all_to_all | solution.py:32
  15.9 1.1 copy.27
  17.0 1.8 pad_maximum_fusion
  18.8 0.9 copy.25
  19.8 34.4 %all-to-all-done = bf16[8,768,256]{1,2,0:T(8,128)(2,1)S(1)} async-done(((bf16[8,768,256]{1,2,0:T(8,128)(2,1)}), bf16[8,768,256]{1,2,0:T(8,128)(2,1)S(1)}, u32[]{:S(2)}, u32[]{:S(2)}) %all-to-all-start) | async-done | bytes 3145760 | tf_op jit(solution)/shard_map/all_to_all | solution.py:32
  54.2 1.1 broadcast_in_dim.7
  55.3 8.9 %all-to-all-start.1 = ((bf16[16,256,128]{1,2,0:T(8,128)(2,1)}), bf16[16,256,128]{1,2,0:T(8,128)(2,1)}, u32[]{:S(2)}, u32[]{:S(2)}) async-start(bf16[16,256,128]{1,2,0:T(8,128)(2,1)} %broadcast_in_dim.7), calls=%async_computation.1 | async-start | bytes 2097152 | tf_op jit(solution)/shard_map/all_to_all | solution.py:32
  64.9 2.5 fusion.3
  67.4 25.0 %all-gather.3.cloned.1.call-done = bf16[2048,512]{1,0:T(8,128)(2,1)} async-done(((bf16[128,512]{1,0:T(8,128)(2,1)}), bf16[2048,512]{1,0:T(8,128)(2,1)}) %all-gather.3.cloned.1.call-update) | async-done | bytes 2097168 | tf_op jit(solution)/shard_map/all_gather | solution.py:45
  92.4 3.2 %fusion.22 = f32[768,256]{1,0:T(8,128)S(1)} fusion(bf16[768,2048]{0,1:T(8,128)(2,1)} %fusion.3, bf16[2048,512]{1,0:T(8,128)(2,1)} %all-gather.3.cloned.1.call-done), kind=kOutput, calls=%fused_computation.35 | convolution fusion | flops 805699584 | bytes 4980736 | tf_op jit(solution)/shard_map/dot_general | solution.py:83
  96.5 0.7 fusion.17
  98.2 1.5 slice.244
  99.6 1.4 slice.248
  101.1 1.2 fusion.65
  102.7 0.7 slice.254
  103.5 1.0 fusion.66
  110.7 0.9 slice.249
  113.4 0.7 fusion.54
  114.8 0.8 fusion.53
  116.9 1.9 pad.77
  118.9 1.9 pad.76
  120.8 6.4 %convolution_convert_fusion = bf16[768,2048]{1,0:T(8,128)(2,1)S(1)} fusion(bf16[256,2048]{0,1:T(8,128)(2,1)} %bitcast.9, bf16[768,2048]{0,1:T(8,128)(2,1)} %fusion.3, bf16[2048,512]{1,0:T(8,128)(2,1)} %all-gather.3.cloned.1.call-done, f32[768,256]{1,0:T(8,128)} %pad.76, f32[768,256]{1,0:T(8,128)} %pad.77), kind=kOutput, calls=%fused_computation.15 | convolution fusion | flops 1614741504 | bytes 9961472 | tf_op jit(solution)/shard_map/dot_general | solution.py:87
  127.5 42.6 %all_to_all.25 = bf16[8,256,768]{1,2,0:T(8,128)(2,1)S(1)} all-to-all(bf16[8,256,768]{1,2,0:T(8,128)(2,1)S(1)} %bitcast.57), channel_id=1, replica_groups=mesh['rep'=2,'fs'=16,'tp'=8] {'tp'}, dimensions={0} | all-to-all | bytes 6291456 | tf_op jit(solution)/shard_map/all_to_all | solution.py:56
  171.6 40.9 %all_to_all.26 = bf16[8,768,256]{1,2,0:T(8,128)(2,1)S(1)} all-to-all(bf16[8,768,256]{1,2,0:T(8,128)(2,1)S(1)} %broadcast_in_dim.16), channel_id=1, replica_groups=mesh['rep'=2,'fs'=16,'tp'=8] {'tp'}, dimensions={0} | all-to-all | bytes 6291456 | tf_op jit(solution)/shard_map/all_to_all | solution.py:32
  213.2 2.5 fusion.1
  215.7 5.9 %all-gather.5.cloned.1.call-done = bf16[2048,2048]{0,1:T(8,128)(2,1)} async-done(((bf16[128,2048]{0,1:T(8,128)(2,1)}), bf16[2048,2048]{0,1:T(8,128)(2,1)}) %all-gather.5.cloned.1.call-update) | async-done | bytes 8388624 | tf_op jit(solution)/shard_map/all_gather | solution.py:14
  221.6 12.9 %fusion.8 = bf16[2048,768]{1,0:T(8,128)(2,1)} fusion(bf16[2048,2048]{0,1:T(8,128)(2,1)} %all-gather.5.cloned.1.call-done, bf16[768,2048]{0,1:T(8,128)(2,1)} %fusion.1), kind=kOutput, calls=%fused_computation.14 | convolution fusion | flops 6446383104 | bytes 14680064 | tf_op jit(solution)/shard_map/dot_general | solution.py:87
  234.5 42.1 %all_to_all.27 = bf16[8,256,768]{2,1,0:T(8,128)(2,1)S(1)} all-to-all(bf16[8,256,768]{2,1,0:T(8,128)(2,1)} %bitcast.59), channel_id=1, replica_groups=mesh['rep'=2,'fs'=16,'tp'=8] {'tp'}, dimensions={0} | all-to-all | bytes 6291456 | tf_op jit(solution)/shard_map/all_to_all | solution.py:56
  277.4 0.8 fusion.40
  (142 shorter events, 15.9 us)
Async XLA Ops:
  6.5 89.4 %copy-start = (bf16[1,256,256]{2,1,0:T(8,128)(2,1)S(1)}, bf16[1,256,256]{2,1,0:T(8,128)(2,1)}, u32[]{:S(2)}) copy-start(bf16[1,256,256]{2,1,0:T(8,128)(2,1)} %param.17) | copy-start | bytes 393220
  6.5 85.8 %all-gather.3.cloned.1.call-start = ((), (), s32[]{:S(2)}) async-start(), calls=%async_computation.5 | async-start | bytes 2228224 | tf_op jit(solution)/shard_map/all_gather | solution.py:45
  11.2 7.6 %copy-start.10 = (f32[256]{0:T(256)S(1)}, f32[256]{0:T(256)}, u32[]{:S(2)}) copy-start(f32[256]{0:T(256)} %param.19) | copy-start | bytes 3076
  11.2 8.6 %copy-start.9 = (bf16[4,256]{1,0:T(4,128)(2,1)S(1)}, bf16[4,256]{1,0:T(4,128)(2,1)}, u32[]{:S(2)}) copy-start(bf16[4,256]{1,0:T(4,128)(2,1)} %param.16) | copy-start | bytes 6148
  11.2 43.0 %all-to-all-start = ((bf16[8,768,256]{1,2,0:T(8,128)(2,1)}), bf16[8,768,256]{1,2,0:T(8,128)(2,1)S(1)}, u32[]{:S(2)}, u32[]{:S(2)}) async-start(bf16[8,768,256]{1,2,0:T(8,128)(2,1)} %broadcast_in_dim.6), calls=%async_computation | async-start | bytes 6291456 | tf_op jit(solution)/shard_map/all_to_all | solution.py:32
  15.8 205.8 %all-gather.5.cloned.1.call-start = ((), (), s32[]{:S(2)}) async-start(), calls=%async_computation.6 | async-start | bytes 8912896 | tf_op jit(solution)/shard_map/all_gather | solution.py:14
  19.8 45.1 %copy-start.7 = (f32[2048]{0:T(1024)S(1)}, f32[2048]{0:T(1024)}, u32[]{:S(2)}) copy-start(f32[2048]{0:T(1024)} %param.13) | copy-start | bytes 24580
  55.3 65.5 %all-to-all-start.1 = ((bf16[16,256,128]{1,2,0:T(8,128)(2,1)}), bf16[16,256,128]{1,2,0:T(8,128)(2,1)}, u32[]{:S(2)}, u32[]{:S(2)}) async-start(bf16[16,256,128]{1,2,0:T(8,128)(2,1)} %broadcast_in_dim.7), calls=%async_computation.1 | async-start | bytes 2097152 | tf_op jit(solution)/shard_map/all_to_all | solution.py:32
  95.5 0.9 copy-start.11
  97.2 15.4 %copy-start.2 = (f32[768,256]{1,0:T(8,128)}, f32[768,256]{1,0:T(8,128)S(1)}, u32[]{:S(2)}) copy-start(f32[768,256]{1,0:T(8,128)S(1)} %fusion.17) | copy-start | bytes 2359300
  111.6 4.9 %copy-start.5 = (f32[95,256]{1,0:T(8,128)S(1)}, f32[95,256]{1,0:T(8,128)}, u32[]{:S(2)}) copy-start(f32[95,256]{1,0:T(8,128)} %slice.255) | copy-start | bytes 291844
  111.6 4.9 %copy-start.6 = (f32[95,256]{1,0:T(8,128)S(1)}, f32[95,256]{1,0:T(8,128)}, u32[]{:S(2)}) copy-start(f32[95,256]{1,0:T(8,128)} %slice.306) | copy-start | bytes 291844
  111.6 5.0 %copy-start.4 = (f32[191,256]{1,0:T(8,128)S(1)}, f32[191,256]{1,0:T(8,128)}, u32[]{:S(2)}) copy-start(f32[191,256]{1,0:T(8,128)} %slice.249) | copy-start | bytes 586756
  116.7 2.2 slice-start
  170.1 1.0 copy-start.3
  212.5 0.7 copy-start.8
  234.5 43.7 %copy-start.1 = (bf16[1,256,256]{2,1,0:T(8,128)(2,1)S(1)}, bf16[1,256,256]{2,1,0:T(8,128)(2,1)}, u32[]{:S(2)}) copy-start(bf16[1,256,256]{2,1,0:T(8,128)(2,1)} %param.17) | copy-start | bytes 393220
Sparse Core Ops, SparseCore 0:
  9.1 83.1 all-gather.2
  94.1 127.4 all-gather.4
where the time goes:
time: 286 us; the launch traced here: 285 us
  blocking collectives  126 us (44%)
  waiting for transfers between devices  65.4 us (23%)
  local copies, waits for them, and re-layouts  23.9 us (8%)
  matrix products  23.7 us (8%)
  other arithmetic  18.9 us (7%)
  between operations  14 us (5%)
  starting transfers between devices  13.5 us (5%)
    all_to_all x2, blocking collectives, sent_and_summed(): lax.all_to_all(blocks, axis, split_axis=0, concat_axis=0, tiled=True)  84.7 us
    all_to_all x1, blocking collectives, from_everyone(): return lax.all_to_all(copies, axis, split_axis=0, concat_axis=0, tiled=True)  40.9 us
    all_to_all x2, waiting for transfers between devices, from_everyone(): return lax.all_to_all(copies, axis, split_axis=0, concat_axis=0, tiled=True)  34.4 us
    all_gather x1, waiting for transfers between devices, side_by_side(): lax.all_gather(both, axis, axis=dim, tiled=True)  25 us
    dot_general x2, matrix products, feature_term(): lax.dot_general(whole_weight, hidden, (((0,), (1,)), ((), ())), preferred...  19.3 us
    all_to_all x2, starting transfers between devices, from_everyone(): return lax.all_to_all(copies, axis, split_axis=0, concat_axis=0, tiled=True)  13.5 us
    slice x57, local copies, waits for them, and re-layouts, recurrence(): _, states = lax.associative_scan(combine, (decay_rate, drive_term), axis=0)  12.1 us
    all_gather x1, waiting for transfers between devices, turned_gather(): filled = lax.all_gather(both, axis, axis=0, tiled=True)  5.94 us
  transfers between devices with their start and end apart: 4, of which 3 were waited for; matrix products, arithmetic and copies ran while one was open for 17% of the time, Pallas kernels for 0%

commit v1 on v0

--- a/solution.py
+++ b/solution.py
@@ -2,6 +2,7 @@
 import jax.numpy as jnp
 from jax import lax
 from jax.sharding import PartitionSpec as P
+from jax.lax import all_to_all, axis_size
 
 NORM_EPSILON = 1e-06
 GATE_SCALE = 8.0
@@ -11,7 +12,12 @@
     turned = [jnp.moveaxis(a, dim, 0) for a, dim in zip(arrays, dims)]
     widths = [t[0].size for t in turned]
     both = jnp.concatenate([t.reshape(-1, w) for t, w in zip(turned, widths)], axis=1)
-    filled = lax.all_gather(both, axis, axis=0, tiled=True)
+    filled = jnp.concatenate(
+        all_to_all(
+            jnp.stack([both] * axis_size(axis), 0), axis_name=axis, split_axis=0, concat_axis=0
+        ),
+        0,
+    )
     blocks = jnp.split(filled, [sum(widths[:k]) for k in range(1, len(widths))], axis=1)
     return tuple(
         (

time: 286 us -> 474 us (1.66)
  the two profiles are of different devices: /device:TPU:6 before, /device:TPU:64 now
where the time goes in v1:
time: 474 us; the launch traced here: 473 us
  waiting for transfers between devices  275 us (58%)
  blocking collectives  84.2 us (18%)
  local copies, waits for them, and re-layouts  30.8 us (6%)
  starting transfers between devices  28.9 us (6%)
  matrix products  24 us (5%)
  other arithmetic  15.8 us (3%)
  between operations  14.2 us (3%)
    all_to_all x1, waiting for transfers between devices, turned_gather(): all_to_all(jnp.stack([both] * axis_size(axis), 0), axis_name=axis, split_...  180 us
    all_to_all x2, blocking collectives, sent_and_summed(): lax.all_to_all(blocks, axis, split_axis=0, concat_axis=0, tiled=True)  84.2 us
    all_to_all x3, waiting for transfers between devices, from_everyone(): return lax.all_to_all(copies, axis, split_axis=0, concat_axis=0, tiled=True)  71.5 us
    all_gather x1, waiting for transfers between devices, side_by_side(): lax.all_gather(both, axis, axis=dim, tiled=True)  23.3 us
    dot_general x2, matrix products, feature_term(): lax.dot_general(whole_weight, hidden, (((0,), (1,)), ((), ())), preferred...  17.5 us
    all_to_all x3, starting transfers between devices, from_everyone(): return lax.all_to_all(copies, axis, split_axis=0, concat_axis=0, tiled=True)  16.3 us
    all_to_all x1, starting transfers between devices, turned_gather(): all_to_all(jnp.stack([both] * axis_size(axis), 0), axis_name=axis, split_...  12.6 us
    slice x57, local copies, waits for them, and re-layouts, recurrence(): _, states = lax.associative_scan(combine, (decay_rate, drive_term), axis=0)  10.3 us
  transfers between devices with their start and end apart: 5, of which 4 were waited for; matrix products, arithmetic and copies ran while one was open for 9% of the time, Pallas kernels for 0%

profile of v1, /device:TPU:64, one launch (start us, length us, event | category | flops | bytes accessed | tf_op | source)
XLA Modules:
  0.0 472.5 jit_solution(6689349311859390379)
XLA Ops:
  6.5 1.6 pad_maximum_fusion.3
  8.1 1.2 copy.27
  9.3 1.8 broadcast_in_dim.6
  11.2 4.6 all-to-all-start
  15.9 38.2 %all-to-all-done = bf16[8,768,256]{1,2,0:T(8,128)(2,1)S(1)} async-done(((bf16[8,768,256]{1,2,0:T(8,128)(2,1)}), bf16[8,768,256]{1,2,0:T(8,128)(2,1)S(1)}, u32[]{:S(2)}, u32[]{:S(2)}) %all-to-all-start) | async-done | bytes 3145760 | tf_op jit(solution)/shard_map/all_to_all | solution.py:38
  54.2 1.1 broadcast_in_dim.7
  55.2 8.0 %all-to-all-start.1 = ((bf16[16,256,128]{1,2,0:T(8,128)(2,1)}), bf16[16,256,128]{1,2,0:T(8,128)(2,1)}, u32[]{:S(2)}, u32[]{:S(2)}) async-start(bf16[16,256,128]{1,2,0:T(8,128)(2,1)} %broadcast_in_dim.7), calls=%async_computation.1 | async-start | bytes 2097152 | tf_op jit(solution)/shard_map/all_to_all | solution.py:38
  64.0 2.4 fusion.3
  66.4 23.3 %all-gather.2.cloned.1.call-done = bf16[2048,512]{1,0:T(8,128)(2,1)} async-done(((bf16[128,512]{1,0:T(8,128)(2,1)}), bf16[2048,512]{1,0:T(8,128)(2,1)}) %all-gather.2.cloned.1.call-update) | async-done | bytes 2097168 | tf_op jit(solution)/shard_map/all_gather | solution.py:51
  89.7 3.2 fusion.22
  93.2 1.4 fusion.74
  95.6 1.9 fusion.17
  97.5 1.6 slice.246
  99.1 1.5 slice.245
  100.5 1.2 fusion.65
  102.9 1.0 fusion.66
  111.8 2.0 pad.76
  113.7 2.0 pad.77
  115.8 6.4 %convolution_convert_fusion = bf16[768,2048]{1,0:T(8,128)(2,1)S(1)} fusion(bf16[256,2048]{0,1:T(8,128)(2,1)} %bitcast.9, bf16[768,2048]{0,1:T(8,128)(2,1)} %fusion.3, bf16[2048,512]{1,0:T(8,128)(2,1)} %all-gather.2.cloned.1.call-done, f32[768,256]{1,0:T(8,128)} %pad.76, f32[768,256]{1,0:T(8,128)} %pad.77), kind=kOutput, calls=%fused_computation.15 | convolution fusion | flops 1614741504 | bytes 9961472 | tf_op jit(solution)/shard_map/dot_general | solution.py:93
  122.4 43.2 %all_to_all.30 = bf16[8,256,768]{1,2,0:T(8,128)(2,1)S(1)} all-to-all(bf16[8,256,768]{1,2,0:T(8,128)(2,1)S(1)} %bitcast.58), channel_id=1, replica_groups=mesh['rep'=2,'fs'=16,'tp'=8] {'tp'}, dimensions={0} | all-to-all | bytes 6291456 | tf_op jit(solution)/shard_map/all_to_all | solution.py:62
  166.9 1.8 broadcast_in_dim.16
  168.7 3.6 all-to-all-start.4
  172.4 1.1 copy.30
  173.5 1.8 pad_maximum_fusion
  175.3 2.1 copy.31
  177.4 33.3 %all-to-all-done.4 = bf16[8,768,256]{1,2,0:T(8,128)(2,1)S(1)} async-done(((bf16[8,768,256]{1,2,0:T(8,128)(2,1)}), bf16[8,768,256]{1,2,0:T(8,128)(2,1)S(1)}, u32[]{:S(2)}, u32[]{:S(2)}) %all-to-all-start.4) | async-done | bytes 3145760 | tf_op jit(solution)/shard_map/all_to_all | solution.py:38
  210.7 5.4 %stack.2 = bf16[16,128,2048]{2,1,0:T(8,128)(2,1)} broadcast(bf16[128,2048]{1,0:T(8,128)(2,1)} %copy.31), dimensions={1,2} | broadcast | bytes 8912896 | tf_op jit(solution)/shard_map/stack | solution.py:17
  216.1 12.6 %all-to-all-start.3 = ((bf16[16,128,2048]{2,1,0:T(8,128)(2,1)}), bf16[16,128,2048]{2,1,0:T(8,128)(2,1)}, u32[]{:S(2)}, u32[]{:S(2)}) async-start(bf16[16,128,2048]{2,1,0:T(8,128)(2,1)} %stack.2), calls=%async_computation.3 | async-start | bytes 16777216 | tf_op jit(solution)/shard_map/all_to_all | solution.py:16
  229.4 2.4 fusion.1
  231.8 179.8 %all-to-all-done.3 = bf16[16,128,2048]{2,1,0:T(8,128)(2,1)} async-done(((bf16[16,128,2048]{2,1,0:T(8,128)(2,1)}), bf16[16,128,2048]{2,1,0:T(8,128)(2,1)}, u32[]{:S(2)}, u32[]{:S(2)}) %all-to-all-start.3) | async-done | bytes 8388640 | tf_op jit(solution)/shard_map/all_to_all | solution.py:16
  411.6 11.1 %fusion.8 = bf16[2048,768]{1,0:T(8,128)(2,1)S(1)} fusion(bf16[2048,2048]{1,0:T(8,128)(2,1)} %bitcast.13, bf16[768,2048]{0,1:T(8,128)(2,1)} %fusion.1), kind=kOutput, calls=%fused_computation.14 | convolution fusion | flops 6446383104 | bytes 14680064 | tf_op jit(solution)/shard_map/dot_general | solution.py:93
  422.8 41.0 %all_to_all.31 = bf16[8,256,768]{2,1,0:T(8,128)(2,1)S(1)} all-to-all(bf16[8,256,768]{2,1,0:T(8,128)(2,1)S(1)} %bitcast.60), channel_id=1, replica_groups=mesh['rep'=2,'fs'=16,'tp'=8] {'tp'}, dimensions={0} | all-to-all | bytes 6291456 | tf_op jit(solution)/shard_map/all_to_all | solution.py:62
  (150 shorter events, 14.7 us)
Async XLA Ops:
  6.5 86.7 %copy-start = (bf16[1,256,256]{2,1,0:T(8,128)(2,1)S(1)}, bf16[1,256,256]{2,1,0:T(8,128)(2,1)}, u32[]{:S(2)}) copy-start(bf16[1,256,256]{2,1,0:T(8,128)(2,1)} %param.17) | copy-start | bytes 393220
  6.5 83.1 %all-gather.2.cloned.1.call-start = ((), (), s32[]{:S(2)}) async-start(), calls=%async_computation.6 | async-start | bytes 2228224 | tf_op jit(solution)/shard_map/all_gather | solution.py:51
  11.1 4.6 copy-start.9
  11.2 4.7 %copy-start.13 = (f32[256]{0:T(256)S(1)}, f32[256]{0:T(256)}, u32[]{:S(2)}) copy-start(f32[256]{0:T(256)} %param.19) | copy-start | bytes 3076
  11.2 4.8 %copy-start.12 = (bf16[4,256]{1,0:T(4,128)(2,1)S(1)}, bf16[4,256]{1,0:T(4,128)(2,1)}, u32[]{:S(2)}) copy-start(bf16[4,256]{1,0:T(4,128)(2,1)} %param.16) | copy-start | bytes 6148
  11.2 43.0 %all-to-all-start = ((bf16[8,768,256]{1,2,0:T(8,128)(2,1)}), bf16[8,768,256]{1,2,0:T(8,128)(2,1)S(1)}, u32[]{:S(2)}, u32[]{:S(2)}) async-start(bf16[8,768,256]{1,2,0:T(8,128)(2,1)} %broadcast_in_dim.6), calls=%async_computation | async-start | bytes 6291456 | tf_op jit(solution)/shard_map/all_to_all | solution.py:38
  15.9 48.0 %copy-start.10 = (f32[2048]{0:T(1024)S(1)}, f32[2048]{0:T(1024)}, u32[]{:S(2)}) copy-start(f32[2048]{0:T(1024)} %param.13) | copy-start | bytes 24580
  55.2 60.5 %all-to-all-start.1 = ((bf16[16,256,128]{1,2,0:T(8,128)(2,1)}), bf16[16,256,128]{1,2,0:T(8,128)(2,1)}, u32[]{:S(2)}, u32[]{:S(2)}) async-start(bf16[16,256,128]{1,2,0:T(8,128)(2,1)} %broadcast_in_dim.7), calls=%async_computation.1 | async-start | bytes 2097152 | tf_op jit(solution)/shard_map/all_to_all | solution.py:38
  92.9 2.7 copy-start.14
  97.5 12.5 %copy-start.4 = (f32[768,256]{1,0:T(8,128)}, f32[768,256]{1,0:T(8,128)S(1)}, u32[]{:S(2)}) copy-start(f32[768,256]{1,0:T(8,128)S(1)} %fusion.17) | copy-start | bytes 2359300
  103.9 1.0 copy-start.6
  104.1 0.8 copy-start.7
  104.2 0.7 copy-start.8
  111.0 0.7 slice-start
  165.6 1.0 copy-start.5
  166.7 2.0 copy-start.2
  168.7 42.0 %all-to-all-start.4 = ((bf16[8,768,256]{1,2,0:T(8,128)(2,1)}), bf16[8,768,256]{1,2,0:T(8,128)(2,1)S(1)}, u32[]{:S(2)}, u32[]{:S(2)}) async-start(bf16[8,768,256]{1,2,0:T(8,128)(2,1)} %broadcast_in_dim.16), calls=%async_computation.4 | async-start | bytes 6291456 | tf_op jit(solution)/shard_map/all_to_all | solution.py:38
  216.1 195.6 %all-to-all-start.3 = ((bf16[16,128,2048]{2,1,0:T(8,128)(2,1)}), bf16[16,128,2048]{2,1,0:T(8,128)(2,1)}, u32[]{:S(2)}, u32[]{:S(2)}) async-start(bf16[16,128,2048]{2,1,0:T(8,128)(2,1)} %stack.2), calls=%async_computation.3 | async-start | bytes 16777216 | tf_op jit(solution)/shard_map/all_to_all | solution.py:16
  228.7 0.7 copy-start.11
  422.8 42.9 %copy-start.1 = (bf16[1,256,256]{2,1,0:T(8,128)(2,1)S(1)}, bf16[1,256,256]{2,1,0:T(8,128)(2,1)}, u32[]{:S(2)}) copy-start(bf16[1,256,256]{2,1,0:T(8,128)(2,1)} %param.17) | copy-start | bytes 393220
  463.8 1.0 copy-start.3
Sparse Core Ops, SparseCore 0:
  9.1 80.5 all-gather.1
